TPU v7x, 32 devices: a whole 2x2x4 slice. The times are simulated.
32 devices in a mesh: sp: 8 (over z, y), tp: 4 (over x, core).
Axes of the slice: x: 2, y: 2, z: 4, core: 2. Of those that a mesh axis runs over, the one named last changes fastest.
Arguments:
- tokens: bfloat16 [4096, 2048], P(('sp', 'tp')), may hold values from -6 to 6
- norm_gain: bfloat16 [2048], replicated, may hold values from 0.099609375 to 1.8984375
- proj_x: bfloat16 [2048, 2048], P('sp', 'tp'), may hold values from -0.125 to 0.125
- gate_projection: bfloat16 [2048, 2048], P('sp', 'tp'), may hold values from -0.125 to 0.125
- conv_taps: bfloat16 [4, 2048], P(None, 'tp'), may hold values from -3 to 3
- gate_recur: bfloat16 [8, 256, 256], P('tp'), may hold values from -0.375 to 0.375
- gate_input: bfloat16 [8, 256, 256], P('tp'), may hold values from -0.375 to 0.375
- decay_param: float32 [2048], P('tp'), may hold values from 4 to 25
- decay_shift: float32 [8, 4096], P('tp', 'sp'), may hold values from -1.3 to 0, as said below
- proj_out: bfloat16 [2048, 2048], P('tp', 'sp'), may hold values from -0.125 to 0.125
Outputs:
- mixed_out: bfloat16 [4096, 2048], P(('sp', 'tp'))
Inputs may be any that keep to these rules, and one draw needn't show every extreme that they name: `decay_shift`: added log-decays, never positive.
All inputs are finite; a program needn't handle non-finite values.
Results may differ from a plain program's by a relative error of at most 0.015.
Values may be sent and summed in bfloat16 or wider, within the bound.
A program may use at most 128 MiB of HBM per device.

v0:
```python
import jax
import jax.numpy as jnp
from jax import lax
from jax.sharding import PartitionSpec as P

HEAD = 256
CONV = 4


def shifted(block, axis, distance):
    devices = range(lax.axis_size(axis))
    route = [(i - distance, i) for i in devices if i - distance in devices]
    return lax.ppermute(block, axis, route)


def carried_in(array, axis, combine, identity):
    size, index = (lax.axis_size(axis), lax.axis_index(axis))
    everything = jax.tree.map(lambda part: lax.all_gather(part, axis), array)
    start = jax.tree.map(
        lambda part, zero: jnp.broadcast_to(jnp.asarray(zero, part.dtype), part.shape),
        array,
        identity,
    )

    def turn(k, before):
        reached = k < index
        new = combine(before, jax.tree.map(lambda part: part[k], everything))
        return jax.tree.map(lambda a, b: jnp.where(reached, a, b), new, before)

    return lax.fori_loop(0, size, turn, start)


def rms_norm(values, norm_gain):
    floats = values.astype(jnp.float32)
    scaled = floats * lax.rsqrt(jnp.mean(floats * floats, axis=-1, keepdims=True) + 1e-06)
    return (scaled * norm_gain.astype(jnp.float32)).astype(jnp.bfloat16)


def combine_pair(earlier, later):
    return (earlier[0] * later[0], later[0] * earlier[1] + later[1])


def on_device(
    tokens,
    norm_gain,
    proj_x,
    gate_projection,
    conv_taps,
    gate_recur,
    gate_input,
    decay_param,
    decay_shift,
    proj_out,
):
    normed = rms_norm(tokens, norm_gain)
    full_x, full_gate = (
        lax.all_gather(proj_x, "sp", axis=0, tiled=True),
        lax.all_gather(gate_projection, "sp", axis=0, tiled=True),
    )
    local_width = proj_x.shape[1]
    piece = lax.all_gather(normed, "tp", axis=0, tiled=True)
    branch_piece = jnp.dot(piece, full_x, preferred_element_type=jnp.float32).astype(jnp.bfloat16)
    gating_piece = jnp.dot(piece, full_gate, preferred_element_type=jnp.float32).astype(
        jnp.bfloat16
    )
    joined = jnp.concatenate([branch_piece, gating_piece], axis=1)
    branch = joined[:, :local_width]
    gating = joined[:, local_width:]
    row_count = branch.shape[0]
    tail_rows = shifted(branch[row_count - CONV + 1 :], "sp", 1)
    extended = jnp.concatenate([tail_rows, branch], axis=0)
    conv_sum = jnp.zeros((row_count, local_width), jnp.float32)
    for tap_index in range(CONV):
        conv_sum = conv_sum + extended[tap_index : tap_index + row_count].astype(
            jnp.float32
        ) * conv_taps[tap_index].astype(jnp.float32)
    conved = conv_sum.astype(jnp.bfloat16)
    head_count = gate_recur.shape[0]
    grouped = conved.reshape(row_count, head_count, HEAD)
    recur = jax.nn.sigmoid(
        jnp.einsum("thi,hij->thj", grouped, gate_recur, preferred_element_type=jnp.float32)
    )
    inlet = jax.nn.sigmoid(
        jnp.einsum("thi,hij->thj", grouped, gate_input, preferred_element_type=jnp.float32)
    )
    decay_rate = jax.nn.softplus(-decay_param).reshape(head_count, HEAD)
    log_decay = (-8.0 * recur * decay_rate[None] + jnp.transpose(decay_shift)[:, :, None]).reshape(
        row_count, local_width
    )
    decay = jnp.exp(log_decay)
    drive = (
        jnp.sqrt(-jnp.expm1(2.0 * log_decay))
        * inlet.reshape(row_count, local_width)
        * conved.astype(jnp.float32)
    )
    identity = (jnp.ones((local_width,), jnp.float32), jnp.zeros((local_width,), jnp.float32))
    cumulative, local_state = lax.associative_scan(combine_pair, (decay, drive), axis=0)
    carried = carried_in(
        (cumulative[row_count - 1], local_state[row_count - 1]), "sp", combine_pair, identity
    )
    states = local_state + cumulative * carried[1][None, :]
    mixed = (states * jax.nn.gelu(gating.astype(jnp.float32))).astype(jnp.bfloat16)
    out_cols = lax.all_gather(proj_out, "sp", axis=1, tiled=True)
    return lax.psum_scatter(
        jnp.dot(mixed, out_cols, preferred_element_type=jnp.float32).astype(jnp.bfloat16),
        "tp",
        scatter_dimension=0,
        tiled=True,
    )


def solution(mesh):
    in_specs = (
        P(("sp", "tp"), None),
        P(),
        P("sp", "tp"),
        P("sp", "tp"),
        P(None, "tp"),
        P("tp", None, None),
        P("tp", None, None),
        P("tp"),
        P("tp", "sp"),
        P("tp", "sp"),
    )
    out_specs = P(("sp", "tp"), None)
    return jax.shard_map(
        on_device, mesh=mesh, in_specs=in_specs, out_specs=out_specs, check_vma=False
    )
```

profile of v0, /device:TPU:0, one launch (start us, length us, event | category | flops | bytes accessed | tf_op | source)
XLA Modules:
  0.0 287.4 jit_solution(4033228351637639462)
XLA Ops:
  6.5 1.3 fusion.11
  7.8 0.7 convert_element_type.51
  8.5 2.0 fusion.13
  10.6 0.7 all-gather.9.cloned.1.call-update
  11.4 0.7 all-gather.11.cloned.1.call-update
  12.1 0.5 all-gather.13.cloned.1.call-update
  12.7 23.3 %all-gather.7.cloned.1.call-done = bf16[512,2048]{1,0:T(8,128)(2,1)} async-done(((bf16[128,2048]{1,0:T(8,128)(2,1)}), bf16[512,2048]{1,0:T(8,128)(2,1)}) %all-gather.7.cloned.1.call-update) | async-done | bytes 2097168 | tf_op jit(solution)/shard_map/all_gather | solution.py:61
  36.0 51.2 %all-gather.9.cloned.1.call-done = bf16[2048,512]{1,0:T(8,128)(2,1)} async-done(((bf16[256,512]{1,0:T(8,128)(2,1)}), bf16[2048,512]{1,0:T(8,128)(2,1)}) %all-gather.9.cloned.1.call-update) | async-done | bytes 2097168 | tf_op jit(solution)/shard_map/all_gather | solution.py:57
  87.3 3.5 %convolution_convert_fusion.2 = bf16[512,512]{1,0:T(8,128)(2,1)S(1)} fusion(bf16[512,2048]{1,0:T(8,128)(2,1)} %all-gather.7.cloned.1.call-done, bf16[2048,512]{1,0:T(8,128)(2,1)} %all-gather.9.cloned.1.call-done), kind=kOutput, calls=%fused_computation.24 | convolution fusion | flops 1074003968 | bytes 4718592 | tf_op jit(solution)/shard_map/dot_general | solution.py:62
  90.7 2.5 collective-permute-start
  93.3 1.2 collective-permute-done
  94.5 0.5 add_convert_fusion
  95.1 0.6 fusion.49
  95.8 0.4 copy-done.11
  96.2 1.9 fusion.4
  98.1 1.6 copy.31
  99.7 1.2 convert_multiply_fusion.5
  100.9 2.3 slice.367
  103.2 2.1 slice.305
  105.3 2.1 slice.304
  107.5 19.5 %slice.303 = f32[256,512]{0,1:T(8,128)S(1)} slice(f32[512,512]{0,1:T(8,128)S(1)} %bitcast.49), slice={[1:512:2], [0:512:1]} | slice | bytes 1048576 | tf_op jit(solution)/shard_map/slice | solution.py:97
  127.0 19.4 %slice.302 = f32[255,512]{0,1:T(8,128)S(1)} slice(f32[512,512]{0,1:T(8,128)S(1)} %bitcast.50), slice={[2:512:2], [0:512:1]} | slice | bytes 1044480 | tf_op jit(solution)/shard_map/slice | solution.py:97
  146.4 19.5 %slice.307 = f32[256,512]{0,1:T(8,128)S(1)} slice(f32[512,512]{0,1:T(8,128)S(1)} %bitcast.51), slice={[0:511:2], [0:512:1]} | slice | bytes 1048576 | tf_op jit(solution)/shard_map/slice | solution.py:97
  165.9 1.0 copy.36
  166.9 0.2 copy.37
  167.3 1.3 multiply_add_fusion
  168.5 0.3 slice.365
  168.9 0.3 slice.311
  169.2 0.3 slice.310
  169.6 0.3 slice.313
  169.9 0.3 slice.309
  170.2 0.3 slice.308
  170.7 0.2 slice.363
  171.3 0.4 slice.314
  172.7 1.0 copy.35
  175.7 0.9 copy-done.5
  176.7 1.2 fusion.25
  177.9 2.9 pad.144
  180.8 2.7 pad.126
  183.6 2.7 pad.127
  186.3 0.7 add_bitcast_fusion
  187.0 27.3 %all-gather.1 = f32[8,1,512]{2,1,0:T(1,128)S(1)} all-gather(f32[1,1,512]{2,1,0:T(1,128)S(1)} %add_bitcast_fusion), channel_id=1, replica_groups=mesh['sp'=8,'tp'=4] {'sp'}, dimensions={0}, use_global_device_ids=true | all-gather | bytes 18432 | tf_op jit(solution)/shard_map/all_gather | solution.py:18
  214.3 2.8 pad.145
  217.1 0.7 add_bitcast_fusion.1
  217.8 26.1 %all-gather = f32[8,1,512]{2,1,0:T(1,128)S(1)} all-gather(f32[1,1,512]{2,1,0:T(1,128)S(1)} %add_bitcast_fusion.1), channel_id=1, replica_groups=mesh['sp'=8,'tp'=4] {'sp'}, dimensions={0}, use_global_device_ids=true | all-gather | bytes 18432 | tf_op jit(solution)/shard_map/all_gather | solution.py:18
  243.9 0.4 while.14
  244.4 7.9 %convolution_convert_fusion = bf16[512,2048]{1,0:T(8,128)(2,1)} fusion(bf16[512,2048]{1,0:T(8,128)(2,1)} %all-gather.13.cloned.1.call-done, bf16[512,2048]{1,0:T(8,128)(2,1)} %all-gather.7.cloned.1.call-done, bf16[2048,512]{1,0:T(8,128)(2,1)} %all-gather.11.cloned.1.call-done, f32[512,512]{1,0:T(8,128)S(1)} %copy-done.8, f32[512,512]{1,0:T(8,128)} %pad.145, ...), kind=kOutput, calls=%fused_computation.3 | convolution fusion | flops 2152726528 | bytes 12584960 | tf_op jit(solution)/shard_map/dot_general | solution.py:105
  252.3 28.5 %reduce-scatter.2.cloned.1.call-done = bf16[128,2048]{1,0:T(8,128)(2,1)} async-done(((bf16[512,2048]{1,0:T(8,128)(2,1)}), bf16[128,2048]{1,0:T(8,128)(2,1)}) %reduce-scatter.2.cloned.1.call-update) | async-done | bytes 524304 | tf_op jit(solution)/shard_map/reduce_scatter | solution.py:104
  (178 shorter events, 4.0 us)
Async XLA Ops:
  6.5 88.5 %copy-start = (bf16[2,256,256]{2,1,0:T(8,128)(2,1)S(1)}, bf16[2,256,256]{2,1,0:T(8,128)(2,1)}, u32[]{:S(2)}) copy-start(bf16[2,256,256]{2,1,0:T(8,128)(2,1)} %param.17) | copy-start | bytes 786436
  6.5 6.1 %copy-start.9 = (bf16[4,512]{1,0:T(4,128)(2,1)S(1)}, bf16[4,512]{1,0:T(4,128)(2,1)}, u32[]{:S(2)}) copy-start(bf16[4,512]{1,0:T(4,128)(2,1)} %param.16) | copy-start | bytes 12292
  6.5 29.5 %all-gather.7.cloned.1.call-start = ((), (), s32[]{:S(2)}) async-start(), calls=%async_computation.1 | async-start | bytes 2621440 | tf_op jit(solution)/shard_map/all_gather | solution.py:61
  10.6 76.7 %all-gather.9.cloned.1.call-start = ((), (), s32[]{:S(2)}) async-start(), calls=%async_computation.2 | async-start | bytes 2359296 | tf_op jit(solution)/shard_map/all_gather | solution.py:57
  11.3 233.0 %all-gather.11.cloned.1.call-start = ((), (), s32[]{:S(2)}) async-start(), calls=%async_computation.3 | async-start | bytes 2359296 | tf_op jit(solution)/shard_map/all_gather | solution.py:58
  12.1 232.3 %all-gather.13.cloned.1.call-start = ((), (), s32[]{:S(2)}) async-start(), calls=%async_computation.4 | async-start | bytes 2359296 | tf_op jit(solution)/shard_map/all_gather | solution.py:103
  12.6 268.2 %reduce-scatter.2.cloned.1.call-start = ((), (), s32[]{:S(2)}) async-start(), calls=%async_computation.5 | async-start | bytes 2621440 | tf_op jit(solution)/shard_map/reduce_scatter | solution.py:104
  12.7 80.5 %copy-start.10 = (f32[512]{0:T(512)S(1)}, f32[512]{0:T(512)}, u32[]{:S(2)}) copy-start(f32[512]{0:T(512)} %param.19) | copy-start | bytes 6148
  12.7 82.3 %copy-start.12 = (f32[2,512]{1,0:T(2,128)S(1)}, f32[2,512]{1,0:T(2,128)}, u32[]{:S(2)}) copy-start(f32[2,512]{1,0:T(2,128)} %param.20) | copy-start | bytes 12292
  90.7 3.8 %collective-permute-start = (bf16[3,512]{1,0:T(4,128)(2,1)S(1)}, bf16[3,512]{1,0:T(4,128)(2,1)S(1)}, u32[]{:S(2)}, u32[]{:S(2)}) collective-permute-start(bf16[3,512]{1,0:T(4,128)(2,1)S(1)} %slice.388), channel_id=1, source_target_pairs={{0,4},{4,8},{8,12},{12,16},{16,20},{20,24},{24,28},{1,5},{5,9},{9,... | collective-permute-start | bytes 9224 | tf_op jit(solution)/shard_map/ppermute | solution.py:13
  95.0 0.8 copy-start.2
  95.1 1.1 copy-start.11
  100.9 26.1 %copy-start.1 = (f32[512,512]{1,0:T(8,128)}, f32[512,512]{1,0:T(8,128)S(1)}, u32[]{:S(2)}) copy-start(f32[512,512]{1,0:T(8,128)S(1)} %convert_multiply_fusion.5) | copy-start | bytes 3145732
  165.9 1.3 copy-start.3
  165.9 1.4 copy-start.4
  175.5 1.1 copy-start.5
  175.5 1.2 copy-start.6
  177.8 2.9 %slice-start = ((f32[512,512]{1,0:T(8,128)}), f32[1,512]{1,0:T(1,128)S(1)}, s32[]{:S(2)}) async-start(f32[512,512]{1,0:T(8,128)} %copy-done.1), calls=%async_computation.6 | async-start | bytes 4096 | tf_op jit(solution)/shard_map/slice | solution.py:97
  177.8 2.9 %copy-start.7 = (f32[255,512]{1,0:T(8,128)S(1)}, f32[255,512]{1,0:T(8,128)}, u32[]{:S(2)}) copy-start(f32[255,512]{1,0:T(8,128)} %get-tuple-element.130) | copy-start | bytes 1566724
  180.8 36.3 %copy-start.8 = (f32[512,512]{1,0:T(8,128)S(1)}, f32[512,512]{1,0:T(8,128)}, u32[]{:S(2)}) copy-start(f32[512,512]{1,0:T(8,128)} %pad.144) | copy-start | bytes 3145732
Sparse Core Ops, SparseCore 0:
  10.7 25.2 all-gather.6
  38.1 49.0 all-gather.8
  89.4 47.6 all-gather.10
  139.0 48.8 all-gather.12
  252.4 28.3 reduce-scatter.1
where the time goes:
time: 288 us; the launch traced here: 287 us
  waiting for transfers between devices  106 us (37%)
  local copies, waits for them, and re-layouts  85.9 us (30%)
  blocking collectives  53.4 us (19%)
  between operations  14.1 us (5%)
  matrix products  13.9 us (5%)
  other arithmetic  10.9 us (4%)
    slice x61, local copies, waits for them, and re-layouts, on_device(): lax.associative_scan(combine_pair, (decay, drive), axis=0)  68.6 us
    all_gather x2, blocking collectives, carried_in(): everything = jax.tree.map(lambda part: lax.all_gather(part, axis), array)  53.4 us
    all_gather x1, waiting for transfers between devices, on_device(): lax.all_gather(proj_x, 'sp', axis=0, tiled=True)  51.2 us
    reduce_scatter x1, waiting for transfers between devices, on_device(): lax.psum_scatter(jnp.dot(mixed, out_cols, preferred_element_type=jnp.floa...  28.5 us
    all_gather x1, waiting for transfers between devices, on_device(): piece = lax.all_gather(normed, 'tp', axis=0, tiled=True)  23.3 us
    pad x32, local copies, waits for them, and re-layouts, on_device(): lax.associative_scan(combine_pair, (decay, drive), axis=0)  11.7 us
    dot_general x1, matrix products, on_device(): jnp.dot(mixed, out_cols, preferred_element_type=jnp.float32)  7.88 us
  transfers between devices with their start and end apart: 6, of which 4 were waited for; matrix products, arithmetic and copies ran while one was open for 34% of the time, Pallas kernels for 0%

commit v1 on v0

--- a/solution.py
+++ b/solution.py
@@ -5,6 +5,15 @@
 
 HEAD = 256
 CONV = 4
+
+
+def move_the_digits(mine_x, dim_at):
+    return jnp.concatenate(
+        jax.lax.all_to_all(
+            jnp.stack(tuple((mine_x for _ in range(jax.lax.axis_size("sp"))))), "sp", 0, 0
+        ),
+        axis=dim_at,
+    )
 
 
 def shifted(block, axis, distance):
@@ -54,7 +63,7 @@
 ):
     normed = rms_norm(tokens, norm_gain)
     full_x, full_gate = (
-        lax.all_gather(proj_x, "sp", axis=0, tiled=True),
+        move_the_digits(proj_x, dim_at=0),
         lax.all_gather(gate_projection, "sp", axis=0, tiled=True),
     )
     local_width = proj_x.shape[1]

time: 288 us -> 278 us (0.965)
  waiting for transfers between devices: 106 us -> 87.2 us
  starting transfers between devices: 2.62 us -> 10.9 us
    all_gather x1 -> x0, waiting for transfers between devices: 51.2 us -> none  [on_device(): lax.all_gather(proj_x, 'sp', axis=0, tiled=True)]
    all_to_all x0 -> x1, waiting for transfers between devices: none -> 41 us  [move_the_digits(): jax.lax.all_to_all(jnp.stack(tuple((mine_x for _ in range(jax.lax.axis_si...]
    all_gather x1, waiting for transfers between devices: 23.3 us -> 14.8 us  [on_device(): piece = lax.all_gather(normed, 'tp', axis=0, tiled=True)]
    all_to_all x0 -> x1, starting transfers between devices: none -> 7.44 us  [move_the_digits(): jax.lax.all_to_all(jnp.stack(tuple((mine_x for _ in range(jax.lax.axis_si...]
  transfers between devices with their start and end apart: 6 -> 6, of which waited for: 4 -> 4; matrix products, arithmetic and copies ran while one was open for 34% -> 35% of each run, Pallas kernels for 0% -> 0%
where the time goes in v1:
time: 278 us
  local copies, waits for them, and re-layouts  87.5 us (31%)
  waiting for transfers between devices  87.2 us (31%)
  blocking collectives  53.6 us (19%)
  between operations  14.1 us (5%)
  matrix products  13.3 us (5%)
  starting transfers between devices  10.9 us (4%)
  other arithmetic  10.9 us (4%)
    slice x61, local copies, waits for them, and re-layouts, on_device(): lax.associative_scan(combine_pair, (decay, drive), axis=0)  68.6 us
    all_gather x2, blocking collectives, carried_in(): everything = jax.tree.map(lambda part: lax.all_gather(part, axis), array)  53.6 us
    all_to_all x1, waiting for transfers between devices, move_the_digits(): jax.lax.all_to_all(jnp.stack(tuple((mine_x for _ in range(jax.lax.axis_si...  41 us
    reduce_scatter x1, waiting for transfers between devices, on_device(): lax.psum_scatter(jnp.dot(mixed, out_cols, preferred_element_type=jnp.floa...  28.6 us
    all_gather x1, waiting for transfers between devices, on_device(): piece = lax.all_gather(normed, 'tp', axis=0, tiled=True)  14.8 us
    pad x32, local copies, waits for them, and re-layouts, on_device(): lax.associative_scan(combine_pair, (decay, drive), axis=0)  11.7 us
    dot_general x1, matrix products, on_device(): jnp.dot(mixed, out_cols, preferred_element_type=jnp.float32)  7.88 us
    all_to_all x1, starting transfers between devices, move_the_digits(): jax.lax.all_to_all(jnp.stack(tuple((mine_x for _ in range(jax.lax.axis_si...  7.44 us
  transfers between devices with their start and end apart: 6, of which 4 were waited for; matrix products, arithmetic and copies ran while one was open for 35% of the time, Pallas kernels for 0%

profile of v1, /device:TPU:0, one launch (start us, length us, event | category | flops | bytes accessed | tf_op | source)
XLA Modules:
  0.0 277.6 jit_solution(5921983017120593081)
XLA Ops:
  6.5 1.3 fusion.11
  7.8 0.7 convert_element_type.51
  8.5 2.0 fusion.13
  10.6 0.7 all-gather.8.cloned.1.call-update
  11.3 1.6 stack.2
  12.9 7.4 %all-to-all-start = ((bf16[8,256,512]{2,1,0:T(8,128)(2,1)}), bf16[8,256,512]{2,1,0:T(8,128)(2,1)S(1)}, u32[]{:S(2)}, u32[]{:S(2)}) async-start(bf16[8,256,512]{2,1,0:T(8,128)(2,1)} %stack.2), calls=%async_computation | async-start | bytes 4194304 | tf_op jit(solution)/shard_map/all_to_all | solution.py:12
  20.4 0.7 all-gather.10.cloned.1.call-update
  21.2 14.8 %all-gather.6.cloned.1.call-done = bf16[512,2048]{1,0:T(8,128)(2,1)} async-done(((bf16[128,2048]{1,0:T(8,128)(2,1)}), bf16[512,2048]{1,0:T(8,128)(2,1)}) %all-gather.6.cloned.1.call-update) | async-done | bytes 2097168 | tf_op jit(solution)/shard_map/all_gather | solution.py:70
  36.0 41.0 %all-to-all-done = bf16[8,256,512]{2,1,0:T(8,128)(2,1)S(1)} async-done(((bf16[8,256,512]{2,1,0:T(8,128)(2,1)}), bf16[8,256,512]{2,1,0:T(8,128)(2,1)S(1)}, u32[]{:S(2)}, u32[]{:S(2)}) %all-to-all-start) | async-done | bytes 2097184 | tf_op jit(solution)/shard_map/all_to_all | solution.py:12
  77.1 2.8 %convolution_convert_fusion.2 = bf16[512,512]{1,0:T(8,128)(2,1)S(1)} fusion(bf16[512,2048]{1,0:T(8,128)(2,1)} %all-gather.6.cloned.1.call-done, bf16[2048,512]{1,0:T(8,128)(2,1)S(1)} %bitcast.55), kind=kOutput, calls=%fused_computation.24 | convolution fusion | flops 1074003968 | bytes 4718592 | tf_op jit(solution)/shard_map/dot_general | solution.py:71
  79.9 3.4 %collective-permute-start = (bf16[3,512]{1,0:T(4,128)(2,1)S(1)}, bf16[3,512]{1,0:T(4,128)(2,1)S(1)}, u32[]{:S(2)}, u32[]{:S(2)}) collective-permute-start(bf16[3,512]{1,0:T(4,128)(2,1)S(1)} %slice.388), channel_id=1, source_target_pairs={{0,4},{4,8},{8,12},{12,16},{16,20},{20,24},{24,28},{1,5},{5,9},{9,... | collective-permute-start | bytes 9224 | tf_op jit(solution)/shard_map/ppermute | solution.py:22
  83.4 1.3 collective-permute-done
  84.6 0.5 add_convert_fusion
  85.2 0.6 fusion.49
  85.9 0.4 copy-done.12
  86.3 1.9 fusion.4
  88.2 1.6 copy.31
  89.8 1.2 convert_multiply_fusion.5
  91.0 2.3 slice.367
  93.3 2.1 slice.305
  95.4 2.1 slice.304
  97.6 19.5 %slice.303 = f32[256,512]{0,1:T(8,128)S(1)} slice(f32[512,512]{0,1:T(8,128)S(1)} %bitcast.50), slice={[1:512:2], [0:512:1]} | slice | bytes 1048576 | tf_op jit(solution)/shard_map/slice | solution.py:106
  117.1 19.4 %slice.302 = f32[255,512]{0,1:T(8,128)S(1)} slice(f32[512,512]{0,1:T(8,128)S(1)} %bitcast.51), slice={[2:512:2], [0:512:1]} | slice | bytes 1044480 | tf_op jit(solution)/shard_map/slice | solution.py:106
  136.5 19.5 %slice.307 = f32[256,512]{0,1:T(8,128)S(1)} slice(f32[512,512]{0,1:T(8,128)S(1)} %bitcast.52), slice={[0:511:2], [0:512:1]} | slice | bytes 1048576 | tf_op jit(solution)/shard_map/slice | solution.py:106
  156.0 1.0 copy.36
  157.0 0.2 copy.37
  157.4 1.3 multiply_add_fusion
  158.6 0.3 slice.365
  159.0 0.3 slice.311
  159.3 0.3 slice.310
  159.6 0.3 slice.313
  160.0 0.3 slice.309
  160.3 0.3 slice.308
  161.4 0.4 slice.314
  162.8 1.0 copy.35
  165.8 0.8 copy-done.5
  166.8 1.2 fusion.25
  168.0 2.9 %pad.144 = f32[512,512]{1,0:T(8,128)} pad(f32[256,512]{1,0:T(8,128)S(1)} %pad_maximum_fusion.2, f32[]{:T(128)} %constant.42.clone.1), padding=0_1_1x0_0_0 | pad | bytes 1572868 | tf_op jit(solution)/shard_map/pad | solution.py:106
  170.9 2.7 pad.126
  173.6 2.7 pad.127
  176.3 0.7 add_bitcast_fusion
  177.1 27.5 %all-gather.1 = f32[8,1,512]{2,1,0:T(1,128)S(1)} all-gather(f32[1,1,512]{2,1,0:T(1,128)S(1)} %add_bitcast_fusion), channel_id=1, replica_groups=mesh['sp'=8,'tp'=4] {'sp'}, dimensions={0}, use_global_device_ids=true | all-gather | bytes 18432 | tf_op jit(solution)/shard_map/all_gather | solution.py:27
  204.5 2.8 pad.145
  207.3 0.7 add_bitcast_fusion.1
  208.0 26.1 %all-gather = f32[8,1,512]{2,1,0:T(1,128)S(1)} all-gather(f32[1,1,512]{2,1,0:T(1,128)S(1)} %add_bitcast_fusion.1), channel_id=1, replica_groups=mesh['sp'=8,'tp'=4] {'sp'}, dimensions={0}, use_global_device_ids=true | all-gather | bytes 18432 | tf_op jit(solution)/shard_map/all_gather | solution.py:27
  234.1 0.4 while.14
  234.6 7.9 %convolution_convert_fusion = bf16[512,2048]{1,0:T(8,128)(2,1)} fusion(bf16[512,2048]{1,0:T(8,128)(2,1)} %all-gather.10.cloned.1.call-done, bf16[512,2048]{1,0:T(8,128)(2,1)} %all-gather.6.cloned.1.call-done, bf16[2048,512]{1,0:T(8,128)(2,1)} %all-gather.8.cloned.1.call-done, f32[512,512]{1,0:T(8,128)S(1)} %copy-done.8, f32[512,512]{1,0:T(8,128)} %pad.145, ...), kind=kOutput, calls=%fused_computation.3 | convolution fusion | flops 2152726528 | bytes 12584960 | tf_op jit(solution)/shard_map/dot_general | solution.py:114
  242.5 28.6 %reduce-scatter.2.cloned.1.call-done = bf16[128,2048]{1,0:T(8,128)(2,1)} async-done(((bf16[512,2048]{1,0:T(8,128)(2,1)}), bf16[128,2048]{1,0:T(8,128)(2,1)}) %reduce-scatter.2.cloned.1.call-update) | async-done | bytes 524304 | tf_op jit(solution)/shard_map/reduce_scatter | solution.py:113
  (180 shorter events, 4.1 us)
Async XLA Ops:
  6.5 78.6 %copy-start = (bf16[2,256,256]{2,1,0:T(8,128)(2,1)S(1)}, bf16[2,256,256]{2,1,0:T(8,128)(2,1)}, u32[]{:S(2)}) copy-start(bf16[2,256,256]{2,1,0:T(8,128)(2,1)} %param.17) | copy-start | bytes 786436
  6.5 4.8 %copy-start.9 = (bf16[256,512]{1,0:T(8,128)(2,1)S(1)}, bf16[256,512]{1,0:T(8,128)(2,1)}, u32[]{:S(2)}) copy-start(bf16[256,512]{1,0:T(8,128)(2,1)} %param.14) | copy-start | bytes 786436
  6.5 29.5 %all-gather.6.cloned.1.call-start = ((), (), s32[]{:S(2)}) async-start(), calls=%async_computation.2 | async-start | bytes 2621440 | tf_op jit(solution)/shard_map/all_gather | solution.py:70
  10.6 224.0 %all-gather.8.cloned.1.call-start = ((), (), s32[]{:S(2)}) async-start(), calls=%async_computation.3 | async-start | bytes 2359296 | tf_op jit(solution)/shard_map/all_gather | solution.py:67
  12.9 8.2 %copy-start.10 = (bf16[4,512]{1,0:T(4,128)(2,1)S(1)}, bf16[4,512]{1,0:T(4,128)(2,1)}, u32[]{:S(2)}) copy-start(bf16[4,512]{1,0:T(4,128)(2,1)} %param.16) | copy-start | bytes 12292
  12.9 64.1 %all-to-all-start = ((bf16[8,256,512]{2,1,0:T(8,128)(2,1)}), bf16[8,256,512]{2,1,0:T(8,128)(2,1)S(1)}, u32[]{:S(2)}, u32[]{:S(2)}) async-start(bf16[8,256,512]{2,1,0:T(8,128)(2,1)} %stack.2), calls=%async_computation | async-start | bytes 4194304 | tf_op jit(solution)/shard_map/all_to_all | solution.py:12
  20.4 214.3 %all-gather.10.cloned.1.call-start = ((), (), s32[]{:S(2)}) async-start(), calls=%async_computation.4 | async-start | bytes 2359296 | tf_op jit(solution)/shard_map/all_gather | solution.py:112
  21.1 250.0 %reduce-scatter.2.cloned.1.call-start = ((), (), s32[]{:S(2)}) async-start(), calls=%async_computation.5 | async-start | bytes 2621440 | tf_op jit(solution)/shard_map/reduce_scatter | solution.py:113
  77.1 6.3 %copy-start.11 = (f32[512]{0:T(512)S(1)}, f32[512]{0:T(512)}, u32[]{:S(2)}) copy-start(f32[512]{0:T(512)} %param.19) | copy-start | bytes 6148
  77.1 8.1 %copy-start.13 = (f32[2,512]{1,0:T(2,128)S(1)}, f32[2,512]{1,0:T(2,128)}, u32[]{:S(2)}) copy-start(f32[2,512]{1,0:T(2,128)} %param.20) | copy-start | bytes 12292
  79.9 4.7 %collective-permute-start = (bf16[3,512]{1,0:T(4,128)(2,1)S(1)}, bf16[3,512]{1,0:T(4,128)(2,1)S(1)}, u32[]{:S(2)}, u32[]{:S(2)}) collective-permute-start(bf16[3,512]{1,0:T(4,128)(2,1)S(1)} %slice.388), channel_id=1, source_target_pairs={{0,4},{4,8},{8,12},{12,16},{16,20},{20,24},{24,28},{1,5},{5,9},{9,... | collective-permute-start | bytes 9224 | tf_op jit(solution)/shard_map/ppermute | solution.py:22
  85.1 0.8 copy-start.2
  85.2 1.1 copy-start.12
  91.0 26.1 %copy-start.1 = (f32[512,512]{1,0:T(8,128)}, f32[512,512]{1,0:T(8,128)S(1)}, u32[]{:S(2)}) copy-start(f32[512,512]{1,0:T(8,128)S(1)} %convert_multiply_fusion.5) | copy-start | bytes 3145732
  156.0 1.3 copy-start.3
  156.0 1.4 copy-start.4
  165.6 1.0 copy-start.5
  165.6 1.2 copy-start.6
  167.9 2.9 %slice-start = ((f32[512,512]{1,0:T(8,128)}), f32[1,512]{1,0:T(1,128)S(1)}, s32[]{:S(2)}) async-start(f32[512,512]{1,0:T(8,128)} %copy-done.1), calls=%async_computation.6 | async-start | bytes 4096 | tf_op jit(solution)/shard_map/slice | solution.py:106
  167.9 2.9 %copy-start.7 = (f32[255,512]{1,0:T(8,128)S(1)}, f32[255,512]{1,0:T(8,128)}, u32[]{:S(2)}) copy-start(f32[255,512]{1,0:T(8,128)} %get-tuple-element.130) | copy-start | bytes 1566724
  170.9 36.4 %copy-start.8 = (f32[512,512]{1,0:T(8,128)S(1)}, f32[512,512]{1,0:T(8,128)}, u32[]{:S(2)}) copy-start(f32[512,512]{1,0:T(8,128)} %pad.144) | copy-start | bytes 3145732
Sparse Core Ops, SparseCore 0:
  10.7 25.2 all-gather.5
  38.1 60.5 all-gather.7
  100.7 48.9 all-gather.9
  242.6 28.3 reduce-scatter.1
